TPU v7x, 32 devices: a whole 2x2x4 slice. The times are simulated.
32 devices in a mesh: ep: 8 (over z, x), tp: 4 (over y, core).
Axes of the slice: x: 2, y: 2, z: 4, core: 2. Of those that a mesh axis runs over, the one named last changes fastest.
Arguments:
- tokens: bfloat16 [192, 4096], P('ep'), may hold values from -6 to 6
- norm_gain: bfloat16 [4096], replicated, may hold values from 0.099609375 to 1.8984375
- w_query: bfloat16 [4096, 1024], P('ep', 'tp'), may hold values from -0.09375 to 0.09375
- w_key: bfloat16 [4096, 1024], P('ep', 'tp'), may hold values from -0.09375 to 0.09375
- w_value: bfloat16 [4096, 2048], P('ep', 'tp'), may hold values from -0.09375 to 0.09375
- w_rgate: bfloat16 [4096, 2048], P('ep', 'tp'), may hold values from -0.09375 to 0.09375
- w_decay: bfloat16 [4096, 1024], P('ep', 'tp'), may hold values from -0.375 to 0.375
- decay_shift: float32 [192, 1024], P('ep', 'tp'), may hold values from -2 to 0
- state: float32 [192, 8, 128, 256], P('ep', 'tp'), may hold values from -6 to 6
- head_gain: bfloat16 [2048], P('tp'), may hold values from 0.099609375 to 1.8984375
- w_out: bfloat16 [2048, 4096], P('tp', 'ep'), may hold values from -0.125 to 0.125
- ffn_gain: bfloat16 [4096], replicated, may hold values from 0.099609375 to 1.8984375
- w_gate: bfloat16 [8, 4096, 1024], P('ep', None, 'tp'), may hold values from -0.21875 to 0.21875
- w_lin: bfloat16 [8, 4096, 1024], P('ep', None, 'tp'), may hold values from -0.21875 to 0.21875
- w_down: bfloat16 [8, 1024, 4096], P('ep', 'tp'), may hold values from -0.046875 to 0.046875
- expert_ids: int32 [192, 4], P('ep'), may hold values from 0 to 7, all different within a row; in each aligned block of 24 rows (0 to 23, 24 to 47, ...) at most 24 rows name the same one
- route_weight: float32 [192, 4], P('ep'), may hold values from 0.2 to 1
Outputs:
- result: bfloat16 [192, 4096], P('ep')
Inputs may be any that keep to these rules, and one draw needn't show every extreme that they name: `expert_ids`: each row names 4 different experts; among the rows of one index of ep no expert is named more than 24 times, a bound that some block reaches.
All inputs are finite; a program needn't handle non-finite values.
Results may differ from a plain program's by a relative error of at most 0.022.
Values may be sent and summed in bfloat16 or wider, within the bound.
A program may use at most 128 MiB of HBM per device.

v0:
```python
import jax
import jax.numpy as jnp
from jax import lax
from jax.sharding import PartitionSpec as P

eps = 1e-06
tau = 16.0
limit = 7.0
glu_alpha = 1.702


def rms_scale(values, gain):
    meansq = jnp.mean(values * values, axis=-1, keepdims=True)
    return values * lax.rsqrt(meansq + eps) * gain


def activate(gate, linear):
    gate = jnp.minimum(gate, limit)
    linear = jnp.clip(linear, -limit, limit)
    return (gate * jax.nn.sigmoid(glu_alpha * gate) * (linear + 1.0)).astype(jnp.bfloat16)


def on_device(
    tokens,
    norm_gain,
    w_query,
    w_key,
    w_value,
    w_rgate,
    w_decay,
    decay_shift,
    state,
    head_gain,
    w_out,
    ffn_gain,
    w_gate,
    w_lin,
    w_down,
    expert_ids,
    route_weight,
):
    seq_dev = tokens.shape[0]
    width = tokens.shape[1]
    heads_dev = state.shape[1]
    key_dim = state.shape[2]
    val_dim = state.shape[3]
    key_cols = w_query.shape[1]
    val_cols = w_value.shape[1]
    inputs = tokens.astype(jnp.float32)
    normed = rms_scale(inputs, norm_gain.astype(jnp.float32)).astype(jnp.bfloat16)
    spread = lax.all_to_all(normed, "ep", split_axis=1, concat_axis=0, tiled=True)
    joined = jnp.concatenate((w_query, w_key, w_decay, w_value, w_rgate), axis=1)
    projected = lax.psum_scatter(
        jnp.dot(spread, joined, preferred_element_type=jnp.float32),
        "ep",
        scatter_dimension=0,
        tiled=True,
    )
    projected = projected.astype(jnp.bfloat16).astype(jnp.float32)
    q_rows = projected[:, :key_cols].reshape(seq_dev, heads_dev, key_dim) * key_dim ** (-0.5)
    k_rows = projected[:, key_cols : 2 * key_cols].reshape(seq_dev, heads_dev, key_dim)
    decay_pre = projected[:, 2 * key_cols : 3 * key_cols]
    v_rows = projected[:, 3 * key_cols : 3 * key_cols + val_cols].reshape(
        seq_dev, heads_dev, val_dim
    )
    rgates = projected[:, 3 * key_cols + val_cols :].reshape(seq_dev, heads_dev, val_dim)
    log_decay = jax.nn.log_sigmoid(decay_pre) / tau + decay_shift
    new_state = (
        jnp.exp(log_decay.reshape(seq_dev, heads_dev, key_dim))[..., None] * state
        + k_rows[..., None] * v_rows[:, :, None, :]
    )
    read = jnp.einsum("shk,shkv->shv", q_rows, new_state, precision=lax.Precision.HIGHEST)
    gated = rms_scale(
        read, head_gain.astype(jnp.float32).reshape(heads_dev, val_dim)
    ) * jax.nn.silu(rgates)
    gated = gated.reshape(seq_dev, heads_dev * val_dim).astype(jnp.bfloat16)
    partial_value = jnp.dot(
        lax.all_gather(gated, "ep", axis=0, tiled=True), w_out, preferred_element_type=jnp.float32
    )
    summed = lax.psum(partial_value.astype(jnp.bfloat16), "tp")
    mixed = lax.all_to_all(summed, "ep", split_axis=0, concat_axis=1, tiled=True)
    stream = inputs + mixed.astype(jnp.float32)
    ffn_in = rms_scale(stream, ffn_gain.astype(jnp.float32)).astype(jnp.bfloat16)
    n_ep = lax.axis_size("ep")
    exp_dev = w_gate.shape[0]
    experts = exp_dev * n_ep
    top = expert_ids.shape[1]
    capacity = max(2, 2 * seq_dev * top // experts)
    flat_ids = expert_ids.reshape(-1)
    onehot = (flat_ids[:, None] == jnp.arange(experts, dtype=jnp.int32)[None, :]).astype(jnp.int32)
    rank = jnp.sum((jnp.cumsum(onehot, axis=0) - onehot) * onehot, axis=1)
    slot_of = flat_ids * capacity + rank
    dispatch = (
        jnp.arange(experts * capacity, dtype=jnp.int32)[:, None] == slot_of[None, :]
    ).astype(jnp.bfloat16)
    dispatch = jnp.sum(dispatch.reshape(experts * capacity, seq_dev, top), axis=2)
    outbound = jnp.dot(dispatch, ffn_in, preferred_element_type=jnp.float32).astype(jnp.bfloat16)
    outbound = outbound.reshape(experts, capacity, width)
    arrived = lax.all_to_all(outbound, "ep", split_axis=0, concat_axis=0, tiled=True)
    count = arrived.shape[1]
    rows = arrived.reshape(n_ep, exp_dev, count, width)
    gate = jnp.einsum("secd,edh->sech", rows, w_gate, preferred_element_type=jnp.float32)
    linear = jnp.einsum("secd,edh->sech", rows, w_lin, preferred_element_type=jnp.float32)
    act = activate(gate, linear)
    partial_out = jnp.einsum("sech,ehd->secd", act, w_down, preferred_element_type=jnp.float32)
    summed_out = lax.psum(partial_out.astype(jnp.bfloat16), "tp")
    returned = lax.all_to_all(
        summed_out.reshape(n_ep * exp_dev, count, width),
        "ep",
        split_axis=0,
        concat_axis=0,
        tiled=True,
    )
    picked = (
        returned.reshape(experts * capacity, width)[slot_of]
        .astype(jnp.float32)
        .reshape(seq_dev, top, width)
    )
    routed = jnp.sum(picked * route_weight[..., None], axis=1)
    return (stream + routed).astype(jnp.bfloat16)


def solution(mesh):
    placed = (
        P("ep", None),
        P(),
        P("ep", "tp"),
        P("ep", "tp"),
        P("ep", "tp"),
        P("ep", "tp"),
        P("ep", "tp"),
        P("ep", "tp"),
        P("ep", "tp", None, None),
        P("tp"),
        P("tp", "ep"),
        P(),
        P("ep", None, "tp"),
        P("ep", None, "tp"),
        P("ep", "tp", None),
        P("ep", None),
        P("ep", None),
    )
    return jax.shard_map(
        on_device, mesh=mesh, in_specs=placed, out_specs=P("ep", None), check_vma=False
    )
```

profile of v0, /device:TPU:0, one launch (start us, length us, event | category | flops | bytes accessed | tf_op | source)
XLA Modules:
  0.0 322.8 jit_solution(11763685602241706706)
XLA Ops:
  7.4 1.1 fusion.38
  8.5 1.1 fusion.40
  10.3 7.3 %all-to-all-start = ((bf16[24,8,512]{2,0,1:T(8,128)(2,1)}), bf16[24,8,512]{2,0,1:T(8,128)(2,1)S(1)}, u32[]{:S(2)}, u32[]{:S(2)}) async-start(bf16[24,8,512]{2,0,1:T(8,128)(2,1)} %bitcast.95), calls=%async_computation | async-start | bytes 393216 | tf_op jit(solution)/shard_map/all_to_all | solution.py:51
  17.6 1.7 constant_dynamic-update-slice_fusion.4
  19.3 1.7 constant_dynamic-update-slice_fusion.3
  21.0 1.7 constant_dynamic-update-slice_fusion.2
  24.5 1.0 all-to-all-done
  25.5 3.2 fusion.72
  29.0 65.7 %reduce-scatter.2.cloned.1.call-done = f32[24,1792]{1,0:T(8,128)} async-done(((f32[192,1792]{1,0:T(8,128)}), f32[24,1792]{1,0:T(8,128)}) %reduce-scatter.2.cloned.1.call-update) | async-done | bytes 172048 | tf_op jit(solution)/shard_map/reduce_scatter | solution.py:53
  95.8 6.1 %fusion = f32[24,2,1,256]{3,2,1,0:T(1,128)S(1)} fusion(f32[24,2,128,1]{2,3,1,0:T(1,128)S(1)} %bitcast.103, f32[24,2,128,256]{3,2,1,0:T(8,128)} %param.25, f32[24,2,256]{2,1,0:T(2,128)S(1)} %mul.158, f32[24,2,128]{2,1,0:T(2,128)S(1)} %mul.156, f32[24,2,128]{2,1,0:T(2,128)S(1)} %exp.24), kind=kOutput, calls=%fused_computation.1 | convolution fusion | flops 23592960 | bytes 6463488 | tf_op jit(solution)/shard_map/shk,shkv->shv/dot_general | solution.py:72
  102.2 30.6 %all_gather.3 = bf16[192,512]{1,0:T(8,128)(2,1)S(1)} all-gather(bf16[24,512]{1,0:T(8,128)(2,1)S(1)} %bitcast.104), channel_id=1, replica_groups=mesh['ep'=8,'tp'=4] {'ep'}, dimensions={0}, use_global_device_ids=true | all-gather | bytes 221184 | tf_op jit(solution)/shard_map/all_gather | solution.py:78
  132.9 1.0 convolution_convert_fusion.2
  134.1 30.6 %all-reduce.3.cloned.1.call-done = bf16[8,24,512]{2,1,0:T(8,128)(2,1)} async-done(((bf16[8,24,512]{2,1,0:T(8,128)(2,1)}), bf16[8,24,512]{2,1,0:T(8,128)(2,1)}) %all-reduce.3.cloned.1.call-update) | async-done | bytes 196624 | tf_op jit(solution)/shard_map/psum | solution.py:80
  164.6 5.5 %all-to-all-start.1 = ((bf16[8,24,512]{2,1,0:T(8,128)(2,1)}), bf16[8,24,512]{2,1,0:T(8,128)(2,1)S(1)}, u32[]{:S(2)}, u32[]{:S(2)}) async-start(bf16[8,24,512]{2,1,0:T(8,128)(2,1)} %all-reduce.3.cloned.1.call-done), calls=%async_computation.2 | async-start | bytes 393216 | tf_op jit(solution)/shard_map/all_to_all | solution.py:81
  170.7 7.3 %all-to-all-done.1 = bf16[8,24,512]{2,1,0:T(8,128)(2,1)S(1)} async-done(((bf16[8,24,512]{2,1,0:T(8,128)(2,1)}), bf16[8,24,512]{2,1,0:T(8,128)(2,1)S(1)}, u32[]{:S(2)}, u32[]{:S(2)}) %all-to-all-start.1) | async-done | bytes 196640 | tf_op jit(solution)/shard_map/all_to_all | solution.py:81
  178.9 37.3 %all_to_all.42 = bf16[8,24,4096]{2,1,0:T(8,128)(2,1)S(1)} all-to-all(bf16[8,24,4096]{2,1,0:T(8,128)(2,1)S(1)} %bitcast.96), channel_id=1, replica_groups=mesh['ep'=8,'tp'=4] {'ep'}, dimensions={0} | all-to-all | bytes 3145728 | tf_op jit(solution)/shard_map/all_to_all | solution.py:99
  216.2 1.2 copy-done.1
  218.0 5.1 %convolution_convert_fusion = bf16[8,24,4096]{2,1,0:T(8,128)(2,1)} fusion(bf16[1,256,4096]{2,1,0:T(8,128)(2,1)S(1)} %copy-done, bf16[8,24,4096]{2,1,0:T(8,128)(2,1)} %copy-done.1, bf16[1,4096,256]{2,1,0:T(8,128)(2,1)} %param.30, f32[8,1,24,256]{3,2,0,1:T(8,128)S(1)} %fusion.27), kind=kOutput, calls=%fused_computation.5 | convolution fusion | flops 806535168 | bytes 7536640 | tf_op jit(solution)/shard_map/sech,ehd->secd/dot_general | solution.py:105
  223.1 42.3 %all-reduce.5.cloned.1.call-done = bf16[8,24,4096]{2,1,0:T(8,128)(2,1)} async-done(((bf16[8,24,4096]{2,1,0:T(8,128)(2,1)}), bf16[8,24,4096]{2,1,0:T(8,128)(2,1)}) %all-reduce.5.cloned.1.call-update) | async-done | bytes 1572880 | tf_op jit(solution)/shard_map/psum | solution.py:106
  265.5 5.5 %all-to-all-start.3 = ((bf16[8,24,4096]{2,1,0:T(8,128)(2,1)}), bf16[8,24,4096]{2,1,0:T(8,128)(2,1)}, u32[]{:S(2)}, u32[]{:S(2)}) async-start(bf16[8,24,4096]{2,1,0:T(8,128)(2,1)} %all-reduce.5.cloned.1.call-done), calls=%async_computation.4 | async-start | bytes 3145728 | tf_op jit(solution)/shard_map/all_to_all | solution.py:107
  271.2 36.8 %all-to-all-done.3 = bf16[8,24,4096]{2,1,0:T(8,128)(2,1)} async-done(((bf16[8,24,4096]{2,1,0:T(8,128)(2,1)}), bf16[8,24,4096]{2,1,0:T(8,128)(2,1)}, u32[]{:S(2)}, u32[]{:S(2)}) %all-to-all-start.3) | async-done | bytes 1572896 | tf_op jit(solution)/shard_map/all_to_all | solution.py:107
  308.0 3.4 %gather_fusion = bf16[96,4096]{1,0:T(8,128)(2,1)S(1)} fusion(bf16[192,4096]{1,0:T(8,128)(2,1)} %bitcast.22, s32[1024]{0:T(1024)S(1)} %pad_clamp_fusion), kind=kCustom, calls=%fused_computation | custom fusion | bytes 1573248 | tf_op jit(solution)/shard_map/gather | solution.py:115
  311.4 1.6 reshape.151
  313.0 2.5 multiply_reduce_fusion
  (68 shorter events, 8.2 us)
Async XLA Ops:
  6.5 211.5 %copy-start = (bf16[1,256,4096]{2,1,0:T(8,128)(2,1)S(1)}, bf16[1,256,4096]{2,1,0:T(8,128)(2,1)}, u32[]{:S(2)}) copy-start(bf16[1,256,4096]{2,1,0:T(8,128)(2,1)} %param.31) | copy-start | bytes 6291460
  6.5 16.1 %copy-start.5 = (bf16[512,512]{1,0:T(8,128)(2,1)S(1)}, bf16[512,512]{1,0:T(8,128)(2,1)}, u32[]{:S(2)}) copy-start(bf16[512,512]{1,0:T(8,128)(2,1)} %param.21) | copy-start | bytes 1572868
  8.5 15.1 %copy-start.6 = (bf16[512,512]{1,0:T(8,128)(2,1)S(1)}, bf16[512,512]{1,0:T(8,128)(2,1)}, u32[]{:S(2)}) copy-start(bf16[512,512]{1,0:T(8,128)(2,1)} %param.22) | copy-start | bytes 1572868
  10.3 15.2 %all-to-all-start = ((bf16[24,8,512]{2,0,1:T(8,128)(2,1)}), bf16[24,8,512]{2,0,1:T(8,128)(2,1)S(1)}, u32[]{:S(2)}, u32[]{:S(2)}) async-start(bf16[24,8,512]{2,0,1:T(8,128)(2,1)} %bitcast.95), calls=%async_computation | async-start | bytes 393216 | tf_op jit(solution)/shard_map/all_to_all | solution.py:51
  17.6 77.2 %reduce-scatter.2.cloned.1.call-start = ((), (), s32[]{:S(2)}) async-start(), calls=%async_computation.5 | async-start | bytes 1548288 | tf_op jit(solution)/shard_map/reduce_scatter | solution.py:53
  25.5 3.2 %copy-start.11 = (bf16[512]{0:T(512)(128)(2,1)S(1)}, bf16[512]{0:T(512)(128)(2,1)}, u32[]{:S(2)}) copy-start(bf16[512]{0:T(512)(128)(2,1)} %param.26) | copy-start | bytes 3076
  25.5 3.3 %copy-start.9 = (s32[24,4]{0,1:T(4,128)S(1)}, s32[24,4]{0,1:T(4,128)}, u32[]{:S(2)}) copy-start(s32[24,4]{0,1:T(4,128)} %param.32) | copy-start | bytes 1156
  25.5 70.2 %copy-start.7 = (f32[24,256]{1,0:T(8,128)S(1)}, f32[24,256]{1,0:T(8,128)}, u32[]{:S(2)}) copy-start(f32[24,256]{1,0:T(8,128)} %param.24) | copy-start | bytes 73732
  28.7 135.9 %all-reduce.3.cloned.1.call-start = ((), (), s32[]{:S(2)}) async-start(), calls=%async_computation.6 | async-start | bytes 393216 | tf_op jit(solution)/shard_map/psum | solution.py:80
  95.8 37.0 %copy-start.4 = (bf16[512,512]{1,0:T(8,128)(2,1)S(1)}, bf16[512,512]{1,0:T(8,128)(2,1)}, u32[]{:S(2)}) copy-start(bf16[512,512]{1,0:T(8,128)(2,1)} %param.27) | copy-start | bytes 1572868
  101.9 68.7 %copy-start.8 = (bf16[4096]{0:T(1024)(128)(2,1)S(1)}, bf16[4096]{0:T(1024)(128)(2,1)}, u32[]{:S(2)}) copy-start(bf16[4096]{0:T(1024)(128)(2,1)} %param.28) | copy-start | bytes 24580
  102.1 76.0 %copy-start.2 = (bf16[24,4096]{1,0:T(8,128)(2,1)S(1)}, bf16[24,4096]{1,0:T(8,128)(2,1)}, u32[]{:S(2)}) copy-start(bf16[24,4096]{1,0:T(8,128)(2,1)} %param.17) | copy-start | bytes 589828
  164.6 13.3 %all-to-all-start.1 = ((bf16[8,24,512]{2,1,0:T(8,128)(2,1)}), bf16[8,24,512]{2,1,0:T(8,128)(2,1)S(1)}, u32[]{:S(2)}, u32[]{:S(2)}) async-start(bf16[8,24,512]{2,1,0:T(8,128)(2,1)} %all-reduce.3.cloned.1.call-done), calls=%async_computation.2 | async-start | bytes 393216 | tf_op jit(solution)/shard_map/all_to_all | solution.py:81
  170.2 95.3 %all-reduce.5.cloned.1.call-start = ((), (), s32[]{:S(2)}) async-start(), calls=%async_computation.7 | async-start | bytes 3145728 | tf_op jit(solution)/shard_map/psum | solution.py:106
  178.8 38.5 %copy-start.3 = (bf16[1,4096,256]{2,1,0:T(8,128)(2,1)S(1)}, bf16[1,4096,256]{2,1,0:T(8,128)(2,1)}, u32[]{:S(2)}) copy-start(bf16[1,4096,256]{2,1,0:T(8,128)(2,1)} %param.29) | copy-start | bytes 6291460
  216.2 1.2 copy-start.1
  223.1 47.9 %copy-start.10 = (f32[24,4]{0,1:T(4,128)S(1)}, f32[24,4]{0,1:T(4,128)}, u32[]{:S(2)}) copy-start(f32[24,4]{0,1:T(4,128)} %param.33) | copy-start | bytes 1156
  265.5 42.5 %all-to-all-start.3 = ((bf16[8,24,4096]{2,1,0:T(8,128)(2,1)}), bf16[8,24,4096]{2,1,0:T(8,128)(2,1)}, u32[]{:S(2)}, u32[]{:S(2)}) async-start(bf16[8,24,4096]{2,1,0:T(8,128)(2,1)} %all-reduce.5.cloned.1.call-done), calls=%async_computation.4 | async-start | bytes 3145728 | tf_op jit(solution)/shard_map/all_to_all | solution.py:107
Sparse Core Ops, SparseCore 0:
  28.8 65.8 reduce-scatter.1
  134.0 30.6 all-reduce.2
  223.2 42.1 all-reduce.4
where the time goes:
time: 323 us
  waiting for transfers between devices  184 us (57%)
  blocking collectives  68 us (21%)
  starting transfers between devices  18.4 us (6%)
  matrix products  16.5 us (5%)
  local copies, waits for them, and re-layouts  14.5 us (4%)
  between operations  13.4 us (4%)
  other arithmetic  8.18 us (3%)
    reduce_scatter x1, waiting for transfers between devices, on_device(): lax.psum_scatter(jnp.dot(spread, joined, preferred_element_type=jnp.float...  65.7 us
    psum x1, waiting for transfers between devices, on_device(): summed_out = lax.psum(partial_out.astype(jnp.bfloat16), 'tp')  42.3 us
    all_to_all x1, blocking collectives, on_device(): lax.all_to_all(outbound, 'ep', split_axis=0, concat_axis=0, tiled=True)  37.3 us
    all_to_all x1, waiting for transfers between devices, on_device(): lax.all_to_all(summed_out.reshape(n_ep * exp_dev, count, width), 'ep', sp...  36.8 us
    all_gather x1, blocking collectives, on_device(): lax.all_gather(gated, 'ep', axis=0, tiled=True)  30.6 us
    psum x1, waiting for transfers between devices, on_device(): summed = lax.psum(partial_value.astype(jnp.bfloat16), 'tp')  30.6 us
    unnamed x31, local copies, waits for them, and re-layouts  7.35 us
    all_to_all x1, starting transfers between devices, on_device(): lax.all_to_all(normed, 'ep', split_axis=1, concat_axis=0, tiled=True)  7.28 us
  transfers between devices with their start and end apart: 6, of which 6 were waited for; matrix products, arithmetic and copies ran while one was open for 2% of the time, Pallas kernels for 0%

commit v1 on v0

--- a/solution.py
+++ b/solution.py
@@ -1,6 +1,10 @@
+import functools
+
 import jax
 import jax.numpy as jnp
 from jax import lax
+from jax.experimental import pallas as pl
+from jax.experimental.pallas import tpu as pltpu
 from jax.sharding import PartitionSpec as P
 
 eps = 1e-06
@@ -18,6 +22,349 @@
     gate = jnp.minimum(gate, limit)
     linear = jnp.clip(linear, -limit, limit)
     return (gate * jax.nn.sigmoid(glu_alpha * gate) * (linear + 1.0)).astype(jnp.bfloat16)
+
+
+MESH = pl.DeviceIdType.MESH
+
+
+def greet(partners):
+    barrier = pltpu.get_barrier_semaphore()
+    for partner in partners:
+        pl.semaphore_signal(barrier, inc=1, device_id=partner, device_id_type=MESH)
+    pl.semaphore_wait(barrier, len(partners))
+
+
+def remote(src, dst, send, recv, partner):
+    return pltpu.make_async_remote_copy(
+        src_ref=src,
+        dst_ref=dst,
+        send_sem=send,
+        recv_sem=recv,
+        device_id=partner,
+        device_id_type=MESH,
+    )
+
+
+def others(axis, n):
+    me = lax.axis_index(axis)
+    return [{axis: lax.rem(me + k, n)} for k in range(1, n)]
+
+
+def across(axis, distance):
+    me = lax.axis_index(axis)
+    digit = lax.rem(me // distance, 2)
+    return {axis: me + distance - 2 * distance * digit}, digit
+
+
+def digits_of(n):
+    values = []
+    while n > 1:
+        n //= 2
+        values.append(n)
+    return values
+
+
+def comm_call(kernel, ins, out_shape, scratch, number):
+    return pl.pallas_call(
+        kernel,
+        out_shape=out_shape,
+        in_specs=[pl.BlockSpec(memory_space=pltpu.VMEM)] * len(ins),
+        out_specs=jax.tree.map(lambda _: pl.BlockSpec(memory_space=pltpu.VMEM), out_shape),
+        scratch_shapes=scratch,
+        compiler_params=pltpu.CompilerParams(
+            collective_id=number, has_side_effects=True, vmem_limit_bytes=32 * 1024 * 1024
+        ),
+    )(*ins)
+
+
+def token_kernel(n, tok_ref, wt_ref, rows_ref, all_wt_ref, send, recv, send_w, recv_w, local):
+    me = lax.axis_index("ep")
+    span = rows_ref.shape[2]
+    partners = others("ep", n)
+    greet(partners)
+    copies = []
+    for k, partner in enumerate(partners):
+        cols = pl.ds(pl.multiple_of(partner["ep"] * span, span), span)
+        copies.append(
+            remote(tok_ref.at[:, cols], rows_ref.at[me], send.at[k], recv.at[k], partner)
+        )
+        copies.append(remote(wt_ref, all_wt_ref.at[me], send_w.at[k], recv_w.at[k], partner))
+    for copy in copies:
+        copy.start()
+    own = pl.ds(pl.multiple_of(me * span, span), span)
+    keep = pltpu.make_async_copy(tok_ref.at[:, own], rows_ref.at[me], local.at[0])
+    keep_w = pltpu.make_async_copy(wt_ref, all_wt_ref.at[me], local.at[1])
+    keep.start()
+    keep_w.start()
+    keep.wait()
+    keep_w.wait()
+    for copy in copies:
+        copy.wait()
+
+
+def spread_tokens(tokens, weights, n):
+    rows, width = tokens.shape
+    dma = pltpu.SemaphoreType.DMA
+    return comm_call(
+        functools.partial(token_kernel, n),
+        (tokens, weights),
+        (
+            jax.ShapeDtypeStruct((n, rows, width // n), tokens.dtype),
+            jax.ShapeDtypeStruct((n,) + weights.shape, weights.dtype),
+        ),
+        [dma((n - 1,)), dma((n - 1,)), dma((n - 1,)), dma((n - 1,)), dma((2,))],
+        1,
+    )
+
+
+def swap_kernel(n, every, x_ref, out_ref, send, recv, local):
+    me = lax.axis_index("ep")
+    partners = others("ep", n)
+    greet(partners)
+    copies = []
+    for k, partner in enumerate(partners):
+        src = x_ref if every else x_ref.at[partner["ep"]]
+        copies.append(remote(src, out_ref.at[me], send.at[k], recv.at[k], partner))
+    for copy in copies:
+        copy.start()
+    keep = pltpu.make_async_copy(x_ref if every else x_ref.at[me], out_ref.at[me], local)
+    keep.start()
+    keep.wait()
+    for copy in copies:
+        copy.wait()
+
+
+def swap(x, n, every, number):
+    dma = pltpu.SemaphoreType.DMA
+    return comm_call(
+        functools.partial(swap_kernel, n, every),
+        (x,),
+        jax.ShapeDtypeStruct(((n,) + x.shape) if every else x.shape, x.dtype),
+        [dma((n - 1,)), dma((n - 1,)), dma],
+        number,
+    )
+
+
+def stream_kernel(n_ep, n_tp, x_ref, tok_ref, out_ref, land, send_t, recv_t, send, recv):
+    me = lax.axis_index("tp")
+    partners = others("tp", n_tp)
+    stages = [across("ep", d) for d in digits_of(n_ep)]
+    greet(partners + [partner for partner, _ in stages])
+    stages += [across("tp", d) for d in digits_of(n_tp)]
+    copies = [
+        remote(x_ref.at[partner["tp"]], land.at[k], send_t.at[k], recv_t.at[k], partner)
+        for k, partner in enumerate(partners)
+    ]
+    for copy in copies:
+        copy.start()
+    for copy in copies:
+        copy.wait()
+    place = sum(digit * 2**k for k, (_, digit) in enumerate(stages))
+    total = x_ref[me].astype(jnp.float32)
+    for k in range(n_tp - 1):
+        total = total + land[k].astype(jnp.float32)
+    mixed = total.astype(jnp.bfloat16).astype(jnp.float32)
+    out_ref[place] = (tok_ref[...].astype(jnp.float32) + mixed).astype(out_ref.dtype)
+    for k, (partner, _) in enumerate(stages):
+        held = out_ref.at[pl.ds((place // 2**k) * 2**k, 2**k)]
+        copy = remote(held, held, send.at[k], recv.at[k], partner)
+        copy.start()
+        copy.wait()
+
+
+def gather_stream(partial_value, tok, n_ep, n_tp, number):
+    dma = pltpu.SemaphoreType.DMA
+    depth = len(digits_of(n_ep)) + len(digits_of(n_tp))
+    return comm_call(
+        functools.partial(stream_kernel, n_ep, n_tp),
+        (partial_value, tok),
+        jax.ShapeDtypeStruct((n_ep * n_tp,) + tok.shape, jnp.bfloat16),
+        [
+            pltpu.VMEM((n_tp - 1,) + tok.shape, jnp.bfloat16),
+            dma((n_tp - 1,)),
+            dma((n_tp - 1,)),
+            dma((depth,)),
+            dma((depth,)),
+        ],
+        number,
+    )
+
+
+def combine_kernel(n_ep, n_tp, x_ref, out_ref, work, land, send, recv, send_t, recv_t, local):
+    me = lax.axis_index("tp")
+    partners = others("tp", n_tp)
+    ep_stages = [across("ep", d) for d in reversed(digits_of(n_ep))]
+    greet(partners + [partner for partner, _ in ep_stages])
+    stages = [across("tp", d) for d in reversed(digits_of(n_tp))] + ep_stages
+    source, size, at = x_ref, n_ep * n_tp, 0
+    for k, (partner, digit) in enumerate(stages):
+        size //= 2
+        copy = remote(
+            source.at[pl.ds((1 - digit) * size, size)],
+            land.at[pl.ds(at, size)],
+            send.at[k],
+            recv.at[k],
+            partner,
+        )
+        copy.start()
+        copy.wait()
+
+        def add(j, _, source=source, size=size, at=at, digit=digit):
+            both = source[digit * size + j].astype(jnp.float32) + land[at + j].astype(jnp.float32)
+            work[at + j] = both.astype(work.dtype)
+            return 0
+
+        lax.fori_loop(0, size, add, 0)
+        source, at = work.at[pl.ds(at, size)], at + size
+    copies = [
+        remote(source.at[0], out_ref.at[me], send_t.at[k], recv_t.at[k], partner)
+        for k, partner in enumerate(partners)
+    ]
+    for copy in copies:
+        copy.start()
+    keep = pltpu.make_async_copy(source.at[0], out_ref.at[me], local)
+    keep.start()
+    keep.wait()
+    for copy in copies:
+        copy.wait()
+
+
+def combine(blocks, n_ep, n_tp, number):
+    dma = pltpu.SemaphoreType.DMA
+    depth = len(digits_of(n_ep)) + len(digits_of(n_tp))
+    block = blocks.shape[1:]
+    return comm_call(
+        functools.partial(combine_kernel, n_ep, n_tp),
+        (blocks,),
+        jax.ShapeDtypeStruct((n_tp,) + block, jnp.bfloat16),
+        [
+            pltpu.VMEM((n_ep * n_tp - 1,) + block, jnp.bfloat16),
+            pltpu.VMEM((n_ep * n_tp - 1,) + block, jnp.bfloat16),
+            dma((depth,)),
+            dma((depth,)),
+            dma((n_tp - 1,)),
+            dma((n_tp - 1,)),
+            dma,
+        ],
+        number,
+    )
+
+
+def folded(blocks):
+    lead, (rows, cols) = blocks.shape[:-2], blocks.shape[-2:]
+    halves = jnp.swapaxes(blocks.reshape(lead + (rows, 2, cols // 2)), -3, -2)
+    return halves.reshape(lead + (2 * rows, cols // 2))
+
+
+def unfolded(blocks):
+    lead, (rows, cols) = blocks.shape[:-2], blocks.shape[-2:]
+    halves = jnp.swapaxes(blocks.reshape(lead + (2, rows // 2, cols)), -3, -2)
+    return halves.reshape(lead + (rows // 2, 2 * cols))
+
+
+def on_device_dense(
+    tokens,
+    norm_gain,
+    w_query,
+    w_key,
+    w_value,
+    w_rgate,
+    w_decay,
+    decay_shift,
+    state,
+    head_gain,
+    w_out,
+    ffn_gain,
+    w_gate,
+    w_lin,
+    w_down,
+    expert_ids,
+    route_weight,
+):
+    n_ep, n_tp = lax.axis_size("ep"), lax.axis_size("tp")
+    my_ep, my_tp = lax.axis_index("ep"), lax.axis_index("tp")
+    seq_dev, width = tokens.shape
+    heads_dev, key_dim, val_dim = state.shape[1:]
+    key_cols = w_query.shape[1]
+    val_cols = w_value.shape[1]
+    exp_dev = w_gate.shape[0]
+    experts = exp_dev * n_ep
+    seqs = seq_dev * n_ep
+    span = width // n_ep
+    lanes = -(-experts // 128) * 128
+    named = expert_ids[:, :, None] == jnp.arange(lanes, dtype=jnp.int32)
+    weights = jnp.sum(jnp.where(named, route_weight[:, :, None], 0.0), axis=1)
+
+    rows, all_weights = spread_tokens(tokens, weights, n_ep)
+    rows = rows.reshape(seqs, span)
+    gain = lax.dynamic_slice_in_dim(norm_gain, my_ep * span, span).astype(jnp.float32)
+    scaled = (rows.astype(jnp.float32) * gain).astype(jnp.bfloat16)
+    parts = [
+        jnp.dot(scaled, w, preferred_element_type=jnp.float32).astype(jnp.bfloat16)
+        for w in (w_query, w_key, w_decay, w_value, w_rgate)
+    ]
+    joined = jnp.concatenate(parts, axis=1)
+    sums = swap(folded(joined.reshape(n_ep, seq_dev, -1)), n_ep, False, 2)
+    inputs = tokens.astype(jnp.float32)
+    inverse = lax.rsqrt(jnp.mean(inputs * inputs, axis=-1, keepdims=True) + eps)
+    projected = unfolded(jnp.sum(sums.astype(jnp.float32), axis=0)) * inverse
+
+    q_rows = projected[:, :key_cols].reshape(seq_dev, heads_dev, key_dim) * key_dim ** (-0.5)
+    k_rows = projected[:, key_cols : 2 * key_cols].reshape(seq_dev, heads_dev, key_dim)
+    decay_pre = projected[:, 2 * key_cols : 3 * key_cols]
+    v_rows = projected[:, 3 * key_cols : 3 * key_cols + val_cols].reshape(
+        seq_dev, heads_dev, val_dim
+    )
+    rgates = projected[:, 3 * key_cols + val_cols :].reshape(seq_dev, heads_dev, val_dim)
+    log_decay = jax.nn.log_sigmoid(decay_pre) / tau + decay_shift
+    decayed = q_rows * jnp.exp(log_decay.reshape(seq_dev, heads_dev, key_dim))
+    read = (
+        jnp.sum(decayed[..., None] * state, axis=2)
+        + jnp.sum(q_rows * k_rows, axis=-1, keepdims=True) * v_rows
+    )
+    gated = rms_scale(
+        read, head_gain.astype(jnp.float32).reshape(heads_dev, val_dim)
+    ) * jax.nn.silu(rgates)
+    gated = gated.reshape(seq_dev, heads_dev * val_dim).astype(jnp.bfloat16)
+
+    all_gated = swap(gated, n_ep, True, 3).reshape(seqs, heads_dev * val_dim)
+    cols = w_out.shape[1] // n_tp
+    partial_value = jnp.dot(all_gated, w_out, preferred_element_type=jnp.float32)
+    partial_value = partial_value.astype(jnp.bfloat16).reshape(seqs, n_tp, cols).swapaxes(0, 1)
+    own_tokens = lax.dynamic_slice_in_dim(rows, my_tp * cols, cols, axis=1)
+    blocks = gather_stream(partial_value, own_tokens, n_ep, n_tp, 4)
+
+    ep_bits, tp_bits = len(digits_of(n_ep)), len(digits_of(n_tp))
+    bits = ep_bits + tp_bits
+    order = [bits - 1 - k for k in range(bits)]
+    stream = blocks.reshape((2,) * bits + (seqs, cols))
+    stream = stream.transpose([bits] + order + [bits + 1]).reshape(seqs, width)
+    stream = stream.astype(jnp.float32)
+    ffn_in = rms_scale(stream, ffn_gain.astype(jnp.float32)).astype(jnp.bfloat16)
+    own_weights = lax.dynamic_slice_in_dim(
+        all_weights.reshape(seqs, lanes), my_ep * exp_dev, exp_dev, axis=1
+    )
+    total = 0.0
+    for index in range(exp_dev):
+        gate = jnp.dot(ffn_in, w_gate[index], preferred_element_type=jnp.float32)
+        linear = jnp.dot(ffn_in, w_lin[index], preferred_element_type=jnp.float32)
+        act = activate(gate, linear)
+        partial_out = jnp.dot(act, w_down[index], preferred_element_type=jnp.float32)
+        total = total + partial_out * own_weights[:, index : index + 1]
+    total = total.astype(jnp.bfloat16)
+    total = total.reshape((2,) * ep_bits + (seq_dev,) + (2,) * tp_bits + (2, width // n_tp // 2))
+    tp_at = list(range(ep_bits + 1, ep_bits + 1 + tp_bits))
+    moved = tp_at[::-1] + list(range(ep_bits))[::-1]
+    last = ep_bits + 1 + tp_bits
+    total = total.transpose(moved + [last, ep_bits, last + 1])
+    total = total.reshape(n_ep * n_tp, 2 * seq_dev, width // n_tp // 2)
+    routed = unfolded(combine(total, n_ep, n_tp, 5)).swapaxes(0, 1).reshape(seq_dev, width)
+    own_stream = lax.dynamic_slice_in_dim(stream, my_ep * seq_dev, seq_dev, axis=0)
+    return (own_stream + routed.astype(jnp.float32)).astype(jnp.bfloat16)
+
+
+def is_power(n):
+    return n > 1 and n & (n - 1) == 0
 
 
 def on_device(
@@ -121,6 +468,17 @@
 
 
 def solution(mesh):
+    n_ep, n_tp = mesh.shape["ep"], mesh.shape["tp"]
+
+    def chosen(*arrays):
+        seq_dev, top = arrays[15].shape
+        experts = arrays[12].shape[0] * n_ep
+        dense = max(2, 2 * seq_dev * top // experts) >= seq_dev
+        whole = arrays[0].shape[1] % (n_ep * n_tp * 128) == 0 and seq_dev % 8 == 0
+        if dense and whole and is_power(n_ep) and is_power(n_tp):
+            return on_device_dense(*arrays)
+        return on_device(*arrays)
+
     placed = (
         P("ep", None),
         P(),
@@ -141,5 +499,5 @@
         P("ep", None),
     )
     return jax.shard_map(
-        on_device, mesh=mesh, in_specs=placed, out_specs=P("ep", None), check_vma=False
-    )
+        chosen, mesh=mesh, in_specs=placed, out_specs=P("ep", None), check_vma=False
+    )

time: 323 us -> 151 us (0.47)
  waiting for transfers between devices: 184 us -> 0 us
  Pallas kernels: 0 us -> 99.7 us
  blocking collectives: 68 us -> 0 us
  starting transfers between devices: 18.4 us -> 0 us
  between operations: 13.4 us -> 0.37 us
  local copies, waits for them, and re-layouts: 14.5 us -> 25 us
  other arithmetic: 8.18 us -> 11.9 us
  matrix products: 16.5 us -> 13.1 us
    pallas_call x0 -> x5, Pallas kernels: none -> 99.7 us  [comm_call(): pl.pallas_call(kernel, out_shape=out_shape, in_specs=[pl.BlockSpec(memory...]
    psum x2 -> x0, waiting for transfers between devices: 72.9 us -> none  [the longest x1 42.3 us: on_device(): summed_out = lax.psum(partial_out.astype(jnp.bfloat16), 'tp')]
    reduce_scatter x1 -> x0, waiting for transfers between devices: 65.7 us -> none  [on_device(): lax.psum_scatter(jnp.dot(spread, joined, preferred_element_type=jnp.float...]
    all_to_all x3 -> x0, waiting for transfers between devices: 45.1 us -> none  [the longest x1 36.8 us: on_device(): lax.all_to_all(summed_out.reshape(n_ep * exp_dev, count, width), 'ep', sp...]
    all_to_all x1 -> x0, blocking collectives: 37.3 us -> none  [on_device(): lax.all_to_all(outbound, 'ep', split_axis=0, concat_axis=0, tiled=True)]
    all_gather x1 -> x0, blocking collectives: 30.6 us -> none  [on_device(): lax.all_gather(gated, 'ep', axis=0, tiled=True)]
    all_to_all x3 -> x0, starting transfers between devices: 18.3 us -> none  [the longest x1 7.28 us: on_device(): lax.all_to_all(normed, 'ep', split_axis=1, concat_axis=0, tiled=True)]
    convert_element_type x2 -> x7, local copies, waits for them, and re-layouts: 1.67 us -> 16.7 us  [the longest x2 9.62 us: on_device_dense(): stream = stream.astype(jnp.float32)]
  transfers between devices with their start and end apart: 6 -> 0, of which waited for: 6 -> 0; matrix products, arithmetic and copies ran while one was open for 2% -> 0% of each run, Pallas kernels for 0% -> 0%
where the time goes in v1:
time: 151 us; the launch traced here: 150 us
  Pallas kernels  99.7 us (66%)
  local copies, waits for them, and re-layouts  25 us (17%)
  matrix products  13.1 us (9%)
  other arithmetic  11.9 us (8%)
    pallas_call x5, Pallas kernels, comm_call(): pl.pallas_call(kernel, out_shape=out_shape, in_specs=[pl.BlockSpec(memory...  99.7 us
    convert_element_type x2, local copies, waits for them, and re-layouts, on_device_dense(): stream = stream.astype(jnp.float32)  9.62 us
    convert_element_type x2, local copies, waits for them, and re-layouts, on_device_dense(): rms_scale(stream, ffn_gain.astype(jnp.float32)).astype(jnp.bfloat16)  6.6 us
    reshape x2, local copies, waits for them, and re-layouts, on_device_dense(): total.reshape((2,) * ep_bits + (seq_dev,) + (2,) * tp_bits + (2, width //...  5.75 us
    dot_general x5, matrix products, on_device_dense(): jnp.dot(scaled, w, preferred_element_type=jnp.float32).astype(jnp.bfloat16)  5.13 us
    dot_general x1, matrix products, on_device_dense(): jnp.dot(act, w_down[index], preferred_element_type=jnp.float32)  5.06 us
    reduce_sum x1, other arithmetic, on_device_dense(): jnp.sum(decayed[..., None] * state, axis=2)  3.44 us

profile of v1, /device:TPU:0, one launch (start us, length us, event | category | flops | bytes accessed | tf_op | source)
XLA Modules:
  0.0 150.1 jit_solution(1318235408274127433)
XLA Ops:
  0.0 1.2 multiply_reduce_fusion.1
  1.2 0.8 dynamic-slice_convert_fusion
  2.7 0.8 select_reduce_fusion.wt_ref
  4.2 0.9 copy-done.2
  5.1 11.3 %shard_map.163 = (bf16[8,24,512]{2,1,0:T(8,128)(2,1)S(1)}, f32[8,24,128]{2,1,0:T(8,128)S(1)}) custom-call(bf16[24,4096]{1,0:T(8,128)(2,1)S(1)} %copy-done.2, f32[24,128]{1,0:T(8,128)S(1)} %select_reduce_fusion.wt_ref), custom_call_target="tpu_custom_call" | custom-call | tf_op jit(solution)/shard_map/pallas_call | solution.py:68
  16.6 1.2 fusion.28
  17.8 1.2 fusion.29
  19.0 1.2 fusion.30
  20.2 1.3 fusion.11
  22.1 16.2 %shard_map.164 = bf16[8,48,896]{2,1,0:T(8,128)(2,1)S(1)} custom-call(bf16[8,48,896]{2,1,0:T(8,128)(2,1)S(1)} %bitcast.83), custom_call_target="tpu_custom_call" | custom-call | tf_op jit(solution)/shard_map/pallas_call | solution.py:68
  38.8 3.4 %multiply_reduce_fusion = f32[24,2,256]{2,1,0:T(2,128)S(1)} fusion(f32[24,2,128,256]{3,2,1,0:T(8,128)} %param.25, f32[24,2,128]{2,1,0:T(2,128)S(1)} %mul.171), kind=kLoop, calls=%fused_computation | loop fusion | flops 3133440 | bytes 6365184 | tf_op jit(solution)/shard_map/reduce_sum | solution.py:322
  42.7 10.5 %shard_map.165 = bf16[8,24,512]{2,1,0:T(8,128)(2,1)S(1)} custom-call(bf16[24,512]{1,0:T(8,128)(2,1)S(1)} %multiply_convert_fusion.6.x_ref), custom_call_target="tpu_custom_call" | custom-call | tf_op jit(solution)/shard_map/pallas_call | solution.py:68
  53.5 30.9 %shard_map.166 = bf16[32,192,128]{2,1,0:T(8,128)(2,1)S(1)} custom-call(bf16[4,192,128]{2,1,0:T(8,128)(2,1)S(1)} %bitcast.90, bf16[192,128]{1,0:T(8,128)(2,1)S(1)} %constant_dynamic-slice_fusion.1.tok_ref), custom_call_target="tpu_custom_call" | custom-call | tf_op jit(solution)/shard_map/pallas_call | solution.py:68
  85.6 2.8 %copy.67 = bf16[192,2,2,2,2,2,128]{6,5,4,3,2,1,0:T(2,128)(2,1)} copy(bf16[192,2,2,2,2,2,128]{6,0,1,2,3,4,5:T(8,128)(2,1)S(1)} %fusion.4) | data formatting | bytes 3145728 | tf_op jit(solution)/shard_map/convert_element_type | solution.py:343
  88.3 3.9 %convert_element_type.109 = bf16[192,4096]{1,0:T(8,128)(2,1)} reshape(bf16[192,2,2,2,2,2,128]{6,5,4,3,2,1,0:T(2,128)(2,1)} %copy.67) | data formatting | bytes 3145728 | tf_op jit(solution)/shard_map/convert_element_type | solution.py:343
  92.2 2.6 %fusion.13 = f32[192,256]{1,0:T(8,128)S(1)} fusion(bf16[192,4096]{1,0:T(8,128)(2,1)} %convert_element_type.109, bf16[1,4096,256]{2,1,0:T(8,128)(2,1)} %param.29), kind=kOutput, calls=%fused_computation.22 | convolution fusion | flops 402702336 | bytes 3866624 | tf_op jit(solution)/shard_map/dot_general | solution.py:349
  94.8 5.1 %fusion = bf16[192,4096]{1,0:T(8,128)(2,1)} fusion(bf16[1,256,4096]{2,1,0:T(8,128)(2,1)S(1)} %copy-done, f32[192]{0:T(256)S(1)} %bitcast.106, bf16[192,4096]{1,0:T(8,128)(2,1)} %convert_element_type.109, bf16[1,4096,256]{2,1,0:T(8,128)(2,1)} %param.30, f32[192,256]{1,0:T(8,128)S(1)} %fusion.13), kind=kOutput, calls=%fused_computation.2 | convolution fusion | flops 807321600 | bytes 7537408 | tf_op jit(solution)/shard_map/dot_general | solution.py:352
  99.9 3.9 %reshape.133 = bf16[2,2,2,24,2,2,2,512]{7,6,5,4,3,2,1,0:T(2,128)(2,1)} reshape(bf16[192,4096]{1,0:T(8,128)(2,1)} %fusion) | data formatting | bytes 3145728 | tf_op jit(solution)/shard_map/reshape | solution.py:355
  103.7 1.9 %copy.69 = bf16[2,2,2,24,2,2,2,512]{7,3,6,0,1,2,4,5:T(8,128)(2,1)S(1)} copy(bf16[2,2,2,24,2,2,2,512]{7,6,5,4,3,2,1,0:T(2,128)(2,1)} %reshape.133) | data formatting | bytes 3145728 | tf_op jit(solution)/shard_map/reshape | solution.py:355
  105.6 30.8 %shard_map.167 = bf16[4,48,512]{2,1,0:T(8,128)(2,1)S(1)} custom-call(bf16[32,48,512]{2,1,0:T(8,128)(2,1)S(1)} %bitcast.82), custom_call_target="tpu_custom_call" | custom-call | tf_op jit(solution)/shard_map/pallas_call | solution.py:68
  137.0 1.8 %convert_bitcast_fusion = f32[192,2,2,2,2,2,128]{6,0,1,2,3,4,5:T(8,128)S(1)} fusion(bf16[32,192,128]{2,1,0:T(8,128)(2,1)} %copy-done.1), kind=kLoop, calls=%fused_computation.5 | loop fusion | flops 786432 | bytes 4718592 | tf_op jit(solution)/shard_map/convert_element_type | solution.py:342
  138.7 4.1 %copy.65 = f32[192,2,2,2,2,2,128]{6,5,4,3,2,1,0:T(2,128)} copy(f32[192,2,2,2,2,2,128]{6,0,1,2,3,4,5:T(8,128)S(1)} %convert_bitcast_fusion) | data formatting | bytes 6291456 | tf_op jit(solution)/shard_map/convert_element_type | solution.py:342
  142.8 5.5 %reshape.136 = f32[192,4096]{1,0:T(8,128)} reshape(f32[192,2,2,2,2,2,128]{6,5,4,3,2,1,0:T(2,128)} %copy.65) | data formatting | bytes 6291456 | tf_op jit(solution)/shard_map/convert_element_type | solution.py:342
  148.3 1.7 %add_convert_fusion = bf16[24,4096]{1,0:T(8,128)(2,1)} fusion(f32[24,4096]{1,0:T(8,128)S(1)} %bitcast.94, f32[192,4096]{1,0:T(8,128)} %reshape.136, s32[]{:T(128)S(6)} %select_n.25), kind=kLoop, calls=%fused_computation.34 | loop fusion | flops 196608 | bytes 983044 | tf_op jit(solution)/shard_map/convert_element_type | solution.py:363
  (45 shorter events, 4.9 us)
Async XLA Ops:
  0.0 94.8 %copy-start = (bf16[1,256,4096]{2,1,0:T(8,128)(2,1)S(1)}, bf16[1,256,4096]{2,1,0:T(8,128)(2,1)}, u32[]{:S(2)}) copy-start(bf16[1,256,4096]{2,1,0:T(8,128)(2,1)} %param.31) | copy-start | bytes 6291460
  4.2 0.9 copy-start.2
  16.6 4.9 %copy-start.3 = (bf16[512,512]{1,0:T(8,128)(2,1)S(1)}, bf16[512,512]{1,0:T(8,128)(2,1)}, u32[]{:S(2)}) copy-start(bf16[512,512]{1,0:T(8,128)(2,1)} %param.22) | copy-start | bytes 1572868
  22.0 16.6 %copy-start.5 = (f32[24,256]{1,0:T(8,128)S(1)}, f32[24,256]{1,0:T(8,128)}, u32[]{:S(2)}) copy-start(f32[24,256]{1,0:T(8,128)} %param.24) | copy-start | bytes 73732
  38.8 14.4 %copy-start.4 = (bf16[512,512]{1,0:T(8,128)(2,1)S(1)}, bf16[512,512]{1,0:T(8,128)(2,1)}, u32[]{:S(2)}) copy-start(bf16[512,512]{1,0:T(8,128)(2,1)} %param.27) | copy-start | bytes 1572868
  84.4 1.2 copy-start.1

commit v2 on v1

--- a/solution.py
+++ b/solution.py
@@ -145,12 +145,26 @@
     )
 
 
+def axes_of(n_ep, n_tp):
+    return [("ep", d) for d in digits_of(n_ep)] + [("tp", d) for d in digits_of(n_tp)]
+
+
+def orders_of(n_ep, n_tp):
+    count = len(axes_of(n_ep, n_tp))
+    first = list(range(count))
+    second = list(first)
+    if count > 2:
+        second[-3], second[-2] = second[-2], second[-3]
+    return first, second
+
+
 def stream_kernel(n_ep, n_tp, x_ref, tok_ref, out_ref, land, send_t, recv_t, send, recv):
     me = lax.axis_index("tp")
     partners = others("tp", n_tp)
-    stages = [across("ep", d) for d in digits_of(n_ep)]
-    greet(partners + [partner for partner, _ in stages])
-    stages += [across("tp", d) for d in digits_of(n_tp)]
+    axes = axes_of(n_ep, n_tp)
+    pairs = [across(*axis) for axis in axes]
+    digits = tuple(digit for _, digit in pairs)
+    greet(partners + [pair[0] for pair, axis in zip(pairs, axes) if axis[0] == "ep"])
     copies = [
         remote(x_ref.at[partner["tp"]], land.at[k], send_t.at[k], recv_t.at[k], partner)
         for k, partner in enumerate(partners)
@@ -159,107 +173,239 @@
         copy.start()
     for copy in copies:
         copy.wait()
-    place = sum(digit * 2**k for k, (_, digit) in enumerate(stages))
     total = x_ref[me].astype(jnp.float32)
     for k in range(n_tp - 1):
         total = total + land[k].astype(jnp.float32)
     mixed = total.astype(jnp.bfloat16).astype(jnp.float32)
-    out_ref[place] = (tok_ref[...].astype(jnp.float32) + mixed).astype(out_ref.dtype)
-    for k, (partner, _) in enumerate(stages):
-        held = out_ref.at[pl.ds((place // 2**k) * 2**k, 2**k)]
-        copy = remote(held, held, send.at[k], recv.at[k], partner)
+    stream = (tok_ref[...].astype(jnp.float32) + mixed).astype(out_ref.dtype)
+    half = stream.shape[0] // 2
+    for piece in range(2):
+        out_ref[(piece,) + digits] = stream[piece * half : (piece + 1) * half]
+    orders = orders_of(n_ep, n_tp)
+
+    def begin(piece, k):
+        done = orders[piece][:k]
+        place = tuple(slice(None) if i in done else digits[i] for i in range(len(axes)))
+        held = out_ref.at[(piece,) + place]
+        partner = pairs[orders[piece][k]][0]
+        copy = remote(held, held, send.at[piece, k], recv.at[piece, k], partner)
         copy.start()
-        copy.wait()
+        return copy
+
+    running = [begin(0, 0), begin(1, 0)]
+    for k in range(len(axes)):
+        for piece in range(2):
+            running[piece].wait()
+            if k + 1 < len(axes):
+                running[piece] = begin(piece, k + 1)
 
 
 def gather_stream(partial_value, tok, n_ep, n_tp, number):
     dma = pltpu.SemaphoreType.DMA
-    depth = len(digits_of(n_ep)) + len(digits_of(n_tp))
+    depth = len(axes_of(n_ep, n_tp))
+    rows, cols = tok.shape
     return comm_call(
         functools.partial(stream_kernel, n_ep, n_tp),
         (partial_value, tok),
-        jax.ShapeDtypeStruct((n_ep * n_tp,) + tok.shape, jnp.bfloat16),
+        jax.ShapeDtypeStruct((2,) + (2,) * depth + (rows // 2, cols), jnp.bfloat16),
         [
             pltpu.VMEM((n_tp - 1,) + tok.shape, jnp.bfloat16),
             dma((n_tp - 1,)),
             dma((n_tp - 1,)),
-            dma((depth,)),
-            dma((depth,)),
+            dma((2, depth)),
+            dma((2, depth)),
         ],
         number,
     )
 
 
-def combine_kernel(n_ep, n_tp, x_ref, out_ref, work, land, send, recv, send_t, recv_t, local):
+def combine_kernel(n_ep, n_tp, x_ref, out_ref, *scratch):
+    axes = axes_of(n_ep, n_tp)
+    depth = len(axes)
+    lands, works = scratch[:depth], scratch[depth : 2 * depth]
+    send, recv, send_t, recv_t, local = scratch[2 * depth :]
     me = lax.axis_index("tp")
     partners = others("tp", n_tp)
-    ep_stages = [across("ep", d) for d in reversed(digits_of(n_ep))]
-    greet(partners + [partner for partner, _ in ep_stages])
-    stages = [across("tp", d) for d in reversed(digits_of(n_tp))] + ep_stages
-    source, size, at = x_ref, n_ep * n_tp, 0
-    for k, (partner, digit) in enumerate(stages):
-        size //= 2
+    pairs = [across(*axis) for axis in axes]
+    greet(partners + [pair[0] for pair, axis in zip(pairs, axes) if axis[0] == "ep"])
+    orders = [order[::-1] for order in orders_of(n_ep, n_tp)]
+
+    def piece_of(piece, k, digit):
+        done = sorted(orders[piece][:k])
+        at = [i for i in range(depth) if i not in done].index(orders[piece][k])
+        lead = (slice(None),) * at
+        source = x_ref if k == 0 else works[k - 1]
+        return source, (piece,) + lead + (digit,), depth - k - 1 - at
+
+    def begin(piece, k):
+        partner, digit = pairs[orders[piece][k]]
+        source, place, _ = piece_of(piece, k, 1 - digit)
         copy = remote(
-            source.at[pl.ds((1 - digit) * size, size)],
-            land.at[pl.ds(at, size)],
-            send.at[k],
-            recv.at[k],
-            partner,
+            source.at[place], lands[k].at[piece], send.at[piece, k], recv.at[piece, k], partner
         )
         copy.start()
-        copy.wait()
-
-        def add(j, _, source=source, size=size, at=at, digit=digit):
-            both = source[digit * size + j].astype(jnp.float32) + land[at + j].astype(jnp.float32)
-            work[at + j] = both.astype(work.dtype)
-            return 0
-
-        lax.fori_loop(0, size, add, 0)
-        source, at = work.at[pl.ds(at, size)], at + size
-    copies = [
-        remote(source.at[0], out_ref.at[me], send_t.at[k], recv_t.at[k], partner)
-        for k, partner in enumerate(partners)
-    ]
-    for copy in copies:
-        copy.start()
-    keep = pltpu.make_async_copy(source.at[0], out_ref.at[me], local)
-    keep.start()
-    keep.wait()
+        return copy
+
+    running = [begin(0, 0), begin(1, 0)]
+    copies = []
+    for k in range(depth):
+        for piece in range(2):
+            running[piece].wait()
+            source, place, _ = piece_of(piece, k, pairs[orders[piece][k]][1])
+            at = len(place) - 2
+            for block in range(2 ** (depth - k - 1)):
+                index = tuple((block >> i) & 1 for i in reversed(range(depth - k - 1)))
+                full = (piece,) + index[:at] + (place[-1],) + index[at:]
+                both = source[full].astype(jnp.float32)
+                both = both + lands[k][(piece,) + index].astype(jnp.float32)
+                works[k][(piece,) + index] = both.astype(jnp.bfloat16)
+            if k + 1 < depth:
+                running[piece] = begin(piece, k + 1)
+                continue
+            last, goal = works[k].at[piece], out_ref.at[me, piece]
+            for j, partner in enumerate(partners):
+                copy = remote(last, goal, send_t.at[piece, j], recv_t.at[piece, j], partner)
+                copy.start()
+                copies.append(copy)
+            keep = pltpu.make_async_copy(last, goal, local.at[piece])
+            keep.start()
+            copies.append(keep)
     for copy in copies:
         copy.wait()
 
 
 def combine(blocks, n_ep, n_tp, number):
     dma = pltpu.SemaphoreType.DMA
-    depth = len(digits_of(n_ep)) + len(digits_of(n_tp))
-    block = blocks.shape[1:]
+    depth = len(axes_of(n_ep, n_tp))
+    block = blocks.shape[-2:]
+    halves = [
+        pltpu.VMEM((2,) + (2,) * (depth - k - 1) + block, jnp.bfloat16) for k in range(depth)
+    ]
     return comm_call(
         functools.partial(combine_kernel, n_ep, n_tp),
         (blocks,),
-        jax.ShapeDtypeStruct((n_tp,) + block, jnp.bfloat16),
-        [
-            pltpu.VMEM((n_ep * n_tp - 1,) + block, jnp.bfloat16),
-            pltpu.VMEM((n_ep * n_tp - 1,) + block, jnp.bfloat16),
-            dma((depth,)),
-            dma((depth,)),
-            dma((n_tp - 1,)),
-            dma((n_tp - 1,)),
-            dma,
+        jax.ShapeDtypeStruct((n_tp, 2) + block, jnp.bfloat16),
+        halves
+        + halves
+        + [
+            dma((2, depth)),
+            dma((2, depth)),
+            dma((2, n_tp - 1)),
+            dma((2, n_tp - 1)),
+            dma((2,)),
         ],
         number,
     )
 
 
-def folded(blocks):
-    lead, (rows, cols) = blocks.shape[:-2], blocks.shape[-2:]
-    halves = jnp.swapaxes(blocks.reshape(lead + (rows, 2, cols // 2)), -3, -2)
-    return halves.reshape(lead + (2 * rows, cols // 2))
-
-
-def unfolded(blocks):
-    lead, (rows, cols) = blocks.shape[:-2], blocks.shape[-2:]
-    halves = jnp.swapaxes(blocks.reshape(lead + (2, rows // 2, cols)), -3, -2)
-    return halves.reshape(lead + (rows // 2, 2 * cols))
+def read_kernel(heads, key_dim, val_dim, tok_ref, sum_ref, shift_ref, state_ref, gain_ref, out_ref):
+    inputs = tok_ref[...].astype(jnp.float32)
+    inverse = lax.rsqrt(jnp.mean(inputs * inputs, axis=-1, keepdims=True) + eps)
+    total = sum_ref[0].astype(jnp.float32)
+    for k in range(1, sum_ref.shape[0]):
+        total = total + sum_ref[k].astype(jnp.float32)
+    projected = total * inverse
+    keys, vals = heads * key_dim, heads * val_dim
+    for head in range(heads):
+        key_at, val_at = head * key_dim, 3 * keys + head * val_dim
+        q_rows = projected[:, key_at : key_at + key_dim] * key_dim ** (-0.5)
+        k_rows = projected[:, keys + key_at : keys + key_at + key_dim]
+        pre = projected[:, 2 * keys + key_at : 2 * keys + key_at + key_dim]
+        v_rows = projected[:, val_at : val_at + val_dim]
+        rgates = projected[:, val_at + vals : val_at + vals + val_dim]
+        log_sig = jnp.minimum(pre, 0.0) - jnp.log1p(jnp.exp(-jnp.abs(pre)))
+        log_decay = log_sig / tau + shift_ref[:, key_at : key_at + key_dim]
+        decayed = jnp.transpose(q_rows * jnp.exp(log_decay))
+        old = [
+            jnp.sum(decayed[:, s : s + 1] * state_ref[s, head], axis=0, keepdims=True)
+            for s in range(state_ref.shape[0])
+        ]
+        read = jnp.concatenate(old, axis=0)
+        read = read + jnp.sum(q_rows * k_rows, axis=-1, keepdims=True) * v_rows
+        cols = slice(head * val_dim, (head + 1) * val_dim)
+        gated = rms_scale(read, gain_ref[:, cols].astype(jnp.float32))
+        out_ref[:, cols] = (gated * (rgates * jax.nn.sigmoid(rgates))).astype(jnp.bfloat16)
+
+
+def gated_read(tokens, sums, decay_shift, state, head_gain):
+    seq_dev, heads, key_dim, val_dim = state.shape
+    tile = 8
+    n, _, cols = sums.shape
+    return pl.pallas_call(
+        functools.partial(read_kernel, heads, key_dim, val_dim),
+        grid=(seq_dev // tile,),
+        out_shape=jax.ShapeDtypeStruct((seq_dev, heads * val_dim), jnp.bfloat16),
+        in_specs=[
+            pl.BlockSpec((tile, tokens.shape[1]), lambda i: (i, 0)),
+            pl.BlockSpec((n, tile, cols), lambda i: (0, i, 0)),
+            pl.BlockSpec((tile, heads * key_dim), lambda i: (i, 0)),
+            pl.BlockSpec((tile, heads, key_dim, val_dim), lambda i: (i, 0, 0, 0)),
+            pl.BlockSpec((1, heads * val_dim), lambda i: (0, 0)),
+        ],
+        out_specs=pl.BlockSpec((tile, heads * val_dim), lambda i: (i, 0)),
+        compiler_params=pltpu.CompilerParams(vmem_limit_bytes=16 * 1024 * 1024),
+    )(tokens, sums, decay_shift, state, head_gain.reshape(1, -1))
+
+
+def expert_kernel(
+    n_ep, n_tp, blocks_ref, gain_ref, gate_ref, lin_ref, down_ref, wt_ref, out_ref, own_ref, ffn
+):
+    pieces, count, rows, cols = blocks_ref.shape
+    seqs, width = ffn.shape
+    seq_dev = seqs // n_ep
+    me = lax.axis_index("ep")
+    per_piece = n_ep // pieces
+    first = pl.multiple_of(lax.rem(me, per_piece) * seq_dev, 8)
+    for j in range(count):
+        at = slice(j * cols, (j + 1) * cols)
+        own_ref[:, at] = blocks_ref[me // per_piece, j, pl.ds(first, seq_dev), :]
+    for piece in range(pieces):
+        square = jnp.zeros((rows, cols), jnp.float32)
+        for j in range(count):
+            block = blocks_ref[piece, j].astype(jnp.float32)
+            square = square + block * block
+        inverse = lax.rsqrt(jnp.sum(square, axis=-1, keepdims=True) / width + eps)
+        for j in range(count):
+            at = slice(j * cols, (j + 1) * cols)
+            scaled = blocks_ref[piece, j].astype(jnp.float32) * inverse
+            scaled = scaled * gain_ref[:, at].astype(jnp.float32)
+            ffn[piece * rows : (piece + 1) * rows, at] = scaled.astype(jnp.bfloat16)
+    acts = []
+    for index in range(gate_ref.shape[0]):
+        gate = jnp.dot(ffn[...], gate_ref[index], preferred_element_type=jnp.float32)
+        linear = jnp.dot(ffn[...], lin_ref[index], preferred_element_type=jnp.float32)
+        acts.append(activate(gate, linear))
+    span = width // n_tp // 2
+    for quarter in range(n_tp):
+        for piece in range(2):
+            start = (2 * quarter + piece) * span
+            total = jnp.zeros((seqs, span), jnp.float32)
+            for index, act in enumerate(acts):
+                part = jnp.dot(
+                    act,
+                    down_ref[index, :, start : start + span],
+                    preferred_element_type=jnp.float32,
+                )
+                total = total + part * wt_ref[:, index : index + 1]
+            total = total.astype(jnp.bfloat16)
+            for e in range(n_ep):
+                out_ref[piece, e, quarter] = total[e * seq_dev : (e + 1) * seq_dev]
+
+
+def run_experts(blocks, ffn_gain, w_gate, w_lin, w_down, own_weights, n_ep, n_tp, seq_dev):
+    width = ffn_gain.shape[0]
+    vmem = pl.BlockSpec(memory_space=pltpu.VMEM)
+    return pl.pallas_call(
+        functools.partial(expert_kernel, n_ep, n_tp),
+        out_shape=(
+            jax.ShapeDtypeStruct((2, n_ep, n_tp, seq_dev, width // n_tp // 2), jnp.bfloat16),
+            jax.ShapeDtypeStruct((seq_dev, width), jnp.bfloat16),
+        ),
+        in_specs=[vmem] * 6,
+        out_specs=(vmem, vmem),
+        scratch_shapes=[pltpu.VMEM((n_ep * seq_dev, width), jnp.bfloat16)],
+        compiler_params=pltpu.CompilerParams(vmem_limit_bytes=32 * 1024 * 1024),
+    )(blocks, ffn_gain.reshape(1, -1), w_gate, w_lin, w_down, own_weights)
 
 
 def on_device_dense(
@@ -284,9 +430,6 @@
     n_ep, n_tp = lax.axis_size("ep"), lax.axis_size("tp")
     my_ep, my_tp = lax.axis_index("ep"), lax.axis_index("tp")
     seq_dev, width = tokens.shape
-    heads_dev, key_dim, val_dim = state.shape[1:]
-    key_cols = w_query.shape[1]
-    val_cols = w_value.shape[1]
     exp_dev = w_gate.shape[0]
     experts = exp_dev * n_ep
     seqs = seq_dev * n_ep
@@ -304,63 +447,32 @@
         for w in (w_query, w_key, w_decay, w_value, w_rgate)
     ]
     joined = jnp.concatenate(parts, axis=1)
-    sums = swap(folded(joined.reshape(n_ep, seq_dev, -1)), n_ep, False, 2)
-    inputs = tokens.astype(jnp.float32)
-    inverse = lax.rsqrt(jnp.mean(inputs * inputs, axis=-1, keepdims=True) + eps)
-    projected = unfolded(jnp.sum(sums.astype(jnp.float32), axis=0)) * inverse
-
-    q_rows = projected[:, :key_cols].reshape(seq_dev, heads_dev, key_dim) * key_dim ** (-0.5)
-    k_rows = projected[:, key_cols : 2 * key_cols].reshape(seq_dev, heads_dev, key_dim)
-    decay_pre = projected[:, 2 * key_cols : 3 * key_cols]
-    v_rows = projected[:, 3 * key_cols : 3 * key_cols + val_cols].reshape(
-        seq_dev, heads_dev, val_dim
-    )
-    rgates = projected[:, 3 * key_cols + val_cols :].reshape(seq_dev, heads_dev, val_dim)
-    log_decay = jax.nn.log_sigmoid(decay_pre) / tau + decay_shift
-    decayed = q_rows * jnp.exp(log_decay.reshape(seq_dev, heads_dev, key_dim))
-    read = (
-        jnp.sum(decayed[..., None] * state, axis=2)
-        + jnp.sum(q_rows * k_rows, axis=-1, keepdims=True) * v_rows
-    )
-    gated = rms_scale(
-        read, head_gain.astype(jnp.float32).reshape(heads_dev, val_dim)
-    ) * jax.nn.silu(rgates)
-    gated = gated.reshape(seq_dev, heads_dev * val_dim).astype(jnp.bfloat16)
-
-    all_gated = swap(gated, n_ep, True, 3).reshape(seqs, heads_dev * val_dim)
+    sums = swap(joined.reshape(n_ep, seq_dev, -1), n_ep, False, 2)
+    gated = gated_read(tokens, sums, decay_shift, state, head_gain)
+
+    all_gated = swap(gated, n_ep, True, 3).reshape(seqs, -1)
     cols = w_out.shape[1] // n_tp
-    partial_value = jnp.dot(all_gated, w_out, preferred_element_type=jnp.float32)
-    partial_value = partial_value.astype(jnp.bfloat16).reshape(seqs, n_tp, cols).swapaxes(0, 1)
+    partial_value = jnp.stack(
+        [
+            jnp.dot(
+                all_gated, w_out[:, t * cols : (t + 1) * cols], preferred_element_type=jnp.float32
+            ).astype(jnp.bfloat16)
+            for t in range(n_tp)
+        ]
+    )
     own_tokens = lax.dynamic_slice_in_dim(rows, my_tp * cols, cols, axis=1)
     blocks = gather_stream(partial_value, own_tokens, n_ep, n_tp, 4)
-
-    ep_bits, tp_bits = len(digits_of(n_ep)), len(digits_of(n_tp))
-    bits = ep_bits + tp_bits
-    order = [bits - 1 - k for k in range(bits)]
-    stream = blocks.reshape((2,) * bits + (seqs, cols))
-    stream = stream.transpose([bits] + order + [bits + 1]).reshape(seqs, width)
-    stream = stream.astype(jnp.float32)
-    ffn_in = rms_scale(stream, ffn_gain.astype(jnp.float32)).astype(jnp.bfloat16)
+    blocks = blocks.reshape(2, n_ep * n_tp, seqs // 2, cols)
     own_weights = lax.dynamic_slice_in_dim(
         all_weights.reshape(seqs, lanes), my_ep * exp_dev, exp_dev, axis=1
     )
-    total = 0.0
-    for index in range(exp_dev):
-        gate = jnp.dot(ffn_in, w_gate[index], preferred_element_type=jnp.float32)
-        linear = jnp.dot(ffn_in, w_lin[index], preferred_element_type=jnp.float32)
-        act = activate(gate, linear)
-        partial_out = jnp.dot(act, w_down[index], preferred_element_type=jnp.float32)
-        total = total + partial_out * own_weights[:, index : index + 1]
-    total = total.astype(jnp.bfloat16)
-    total = total.reshape((2,) * ep_bits + (seq_dev,) + (2,) * tp_bits + (2, width // n_tp // 2))
-    tp_at = list(range(ep_bits + 1, ep_bits + 1 + tp_bits))
-    moved = tp_at[::-1] + list(range(ep_bits))[::-1]
-    last = ep_bits + 1 + tp_bits
-    total = total.transpose(moved + [last, ep_bits, last + 1])
-    total = total.reshape(n_ep * n_tp, 2 * seq_dev, width // n_tp // 2)
-    routed = unfolded(combine(total, n_ep, n_tp, 5)).swapaxes(0, 1).reshape(seq_dev, width)
-    own_stream = lax.dynamic_slice_in_dim(stream, my_ep * seq_dev, seq_dev, axis=0)
-    return (own_stream + routed.astype(jnp.float32)).astype(jnp.bfloat16)
+    total, own_stream = run_experts(
+        blocks, ffn_gain, w_gate, w_lin, w_down, own_weights, n_ep, n_tp, seq_dev
+    )
+    digits = (2,) * len(axes_of(n_ep, n_tp))
+    routed = combine(total.reshape((2,) + digits + total.shape[-2:]), n_ep, n_tp, 5)
+    routed = jnp.concatenate([routed[t, h] for t in range(n_tp) for h in range(2)], axis=1)
+    return (own_stream.astype(jnp.float32) + routed.astype(jnp.float32)).astype(jnp.bfloat16)
 
 
 def is_power(n):

time: 151 us -> 105 us (0.70)
  local copies, waits for them, and re-layouts: 25 us -> 5.27 us
  other arithmetic: 11.9 us -> 2.37 us
  matrix products: 13.1 us -> 4.85 us
  Pallas kernels: 99.7 us -> 91.8 us
    convert_element_type x7 -> x0, local copies, waits for them, and re-layouts: 16.7 us -> none  [the longest x2 9.62 us: on_device_dense(): stream = stream.astype(jnp.float32)]
    pallas_call x5, Pallas kernels: 99.7 us -> 87.3 us  [comm_call(): pl.pallas_call(kernel, out_shape=out_shape, in_specs=[pl.BlockSpec(memory...]
    dot_general x3 -> x4, matrix products: 7.97 us -> 0.78 us  [on_device_dense(): jnp.dot(all_gated, w_out[:, t * cols:(t + 1) * cols], preferred_element_t...]
    reduce_sum x6 -> x0, other arithmetic: 5.42 us -> none  [the longest x1 3.44 us: on_device_dense(): jnp.sum(decayed[..., None] * state, axis=2)]
    pallas_call x0 -> x2, Pallas kernels: none -> 4.52 us  [the longest x1 2.76 us: gated_read(): pl.pallas_call(functools.partial(read_kernel, heads, key_dim, val_dim), g...]
    reshape x5 -> x2, local copies, waits for them, and re-layouts: 5.83 us -> 1.39 us  [the longest x1 0.71 us: run_experts(): ffn_gain.reshape(1, -1)]
    convert_element_type x5 -> x1, other arithmetic: 4.77 us -> 0.73 us  [on_device_dense(): (own_stream.astype(jnp.float32) + routed.astype(jnp.float32)).astype(jnp....]
    unnamed x16 -> x27, local copies, waits for them, and re-layouts: 1.19 us -> 3.77 us
where the time goes in v2:
time: 105 us
  Pallas kernels  91.8 us (87%)
  local copies, waits for them, and re-layouts  5.27 us (5%)
  matrix products  4.85 us (5%)
  other arithmetic  2.37 us (2%)
    pallas_call x5, Pallas kernels, comm_call(): pl.pallas_call(kernel, out_shape=out_shape, in_specs=[pl.BlockSpec(memory...  87.3 us
    dot_general x5, matrix products, on_device_dense(): jnp.dot(scaled, w, preferred_element_type=jnp.float32).astype(jnp.bfloat16)  4.07 us
    unnamed x27, local copies, waits for them, and re-layouts  3.77 us
    pallas_call x1, Pallas kernels, gated_read(): pl.pallas_call(functools.partial(read_kernel, heads, key_dim, val_dim), g...  2.76 us

profile of v2, /device:TPU:0, one launch (start us, length us, event | category | flops | bytes accessed | tf_op | source)
XLA Modules:
  0.0 104.6 jit_solution(14697509837949545277)
XLA Ops:
  0.0 0.8 dynamic-slice_convert_fusion
  0.8 0.7 reshape.29.gain_ref
  1.5 0.8 select_reduce_fusion.wt_ref
  2.3 0.7 reshape.32.gain_ref
  3.0 0.9 copy-done.5
  4.0 11.3 %shard_map.163 = (bf16[8,24,512]{2,1,0:T(8,128)(2,1)S(1)}, f32[8,24,128]{2,1,0:T(8,128)S(1)}) custom-call(bf16[24,4096]{1,0:T(8,128)(2,1)S(1)} %copy-done.5, f32[24,128]{1,0:T(8,128)S(1)} %select_reduce_fusion.wt_ref), custom_call_target="tpu_custom_call" | custom-call | tf_op jit(solution)/shard_map/pallas_call | solution.py:68
  15.3 0.1 constant_dynamic-slice_fusion.wt_ref
  15.4 1.2 %fusion.2 = bf16[192,1792]{1,0:T(8,128)(2,1)S(1)} fusion(bf16[512,256]{1,0:T(8,128)(2,1)} %param.19, bf16[192,512]{1,0:T(8,128)(2,1)S(1)} %bitcast.46, f32[512]{0:T(512)S(1)} %dynamic-slice_convert_fusion), kind=kOutput, calls=%fused_computation.7 | convolution fusion | flops 50675712 | bytes 559104 | tf_op jit(solution)/shard_map/dot_general | solution.py:446
  16.6 1.2 %fusion.3 = bf16[192,1792]{1,0:T(8,128)(2,1)S(1)} fusion(bf16[192,1792]{1,0:T(8,128)(2,1)S(1)} %fusion.2, bf16[512,256]{1,0:T(8,128)(2,1)} %param.20, bf16[192,512]{1,0:T(8,128)(2,1)S(1)} %bitcast.47, f32[512]{0:T(512)S(1)} %dynamic-slice_convert_fusion), kind=kOutput, calls=%fused_computation.8 | convolution fusion | flops 50675712 | bytes 559104 | tf_op jit(solution)/shard_map/dot_general | solution.py:446
  17.8 1.2 %fusion.4 = bf16[192,1792]{1,0:T(8,128)(2,1)S(1)} fusion(bf16[192,1792]{1,0:T(8,128)(2,1)S(1)} %fusion.3, bf16[512,256]{1,0:T(8,128)(2,1)} %param.23, bf16[192,512]{1,0:T(8,128)(2,1)S(1)} %bitcast.48, f32[512]{0:T(512)S(1)} %dynamic-slice_convert_fusion), kind=kOutput, calls=%fused_computation.9 | convolution fusion | flops 50675712 | bytes 559104 | tf_op jit(solution)/shard_map/dot_general | solution.py:446
  19.0 0.3 fusion.1
  19.3 0.3 fusion
  19.5 16.2 %shard_map.164.sum_ref = bf16[8,24,1792]{2,1,0:T(8,128)(2,1)S(1)} custom-call(bf16[8,24,1792]{2,1,0:T(8,128)(2,1)S(1)} %bitcast.51), custom_call_target="tpu_custom_call" | custom-call | tf_op jit(solution)/shard_map/pallas_call | solution.py:68
  35.8 2.8 %copy-done.1 = f32[24,2,128,256]{3,2,1,0:T(8,128)S(1)} copy-done((f32[24,2,128,256]{3,2,1,0:T(8,128)S(1)}, f32[24,2,128,256]{3,2,1,0:T(8,128)}, u32[]{:S(2)}) %copy-start.1) | copy-done | bytes 6291480
  38.6 2.8 %shard_map.165.x_ref = bf16[24,512]{1,0:T(8,128)(2,1)S(1)} custom-call(bf16[24,4096]{1,0:T(8,128)(2,1)S(1)} %copy-done.6, bf16[8,24,1792]{2,1,0:T(8,128)(2,1)S(1)} %shard_map.164.sum_ref, f32[24,256]{1,0:T(8,128)S(1)} %copy-done.7, f32[24,2,128,256]{3,2,1,0:T(8,128)S(1)} %copy-done.1, bf16[1,512]{1,0:T(2,128)(2,1)S(1)} %reshape.29.gain_ref), custom_call_target="tpu_custom_call" | custom-call | tf_op jit(solution)/shard_map/pallas_call | solution.py:334
  41.4 10.4 %shard_map.166 = bf16[8,24,512]{2,1,0:T(8,128)(2,1)S(1)} custom-call(bf16[24,512]{1,0:T(8,128)(2,1)S(1)} %shard_map.165.x_ref), custom_call_target="tpu_custom_call" | custom-call | tf_op jit(solution)/shard_map/pallas_call | solution.py:68
  51.8 0.2 fusion.8
  52.0 0.2 fusion.7
  52.2 0.2 fusion.6
  52.4 0.2 fusion.5
  52.6 25.2 %shard_map.167 = bf16[2,2,2,2,2,2,96,128]{7,6,5,4,3,2,1,0:T(8,128)(2,1)S(1)} custom-call(bf16[4,192,128]{2,1,0:T(8,128)(2,1)S(1)} %pad_maximum_fusion.x_ref, bf16[192,128]{1,0:T(8,128)(2,1)S(1)} %constant_dynamic-slice_fusion.1.tok_ref), custom_call_target="tpu_custom_call" | custom-call | tf_op jit(solution)/shard_map/pallas_call | solution.py:68
  77.9 1.8 %shard_map.168 = (bf16[2,8,4,24,512]{4,3,2,1,0:T(8,128)(2,1)S(1)}, bf16[24,4096]{1,0:T(8,128)(2,1)S(1)}) custom-call(bf16[2,32,96,128]{3,2,1,0:T(8,128)(2,1)S(1)} %bitcast.39, bf16[1,4096]{1,0:T(2,128)(2,1)S(1)} %reshape.32.gain_ref, bf16[1,4096,256]{2,1,0:T(8,128)(2,1)S(1)} %copy-done.2, bf16[1,4096,256]{2,1,0:T(8,128)(2,1)S(1)} %copy-done.3, ...), custom_call_target="tpu_custom_call" | custom-call | tf_op jit(solution)/shard_map/pallas_call | solution.py:398
  79.6 24.1 %shard_map.169 = bf16[4,2,24,512]{3,2,1,0:T(8,128)(2,1)S(1)} custom-call(bf16[2,2,2,2,2,2,24,512]{7,6,5,4,3,2,1,0:T(8,128)(2,1)S(1)} %bitcast.44), custom_call_target="tpu_custom_call" | custom-call | tf_op jit(solution)/shard_map/pallas_call | solution.py:68
  103.9 0.7 add_convert_fusion
  (28 shorter events, 0.1 us)
Async XLA Ops:
  0.0 19.0 %copy-start = (bf16[512,512]{1,0:T(8,128)(2,1)S(1)}, bf16[512,512]{1,0:T(8,128)(2,1)}, u32[]{:S(2)}) copy-start(bf16[512,512]{1,0:T(8,128)(2,1)} %param.21) | copy-start | bytes 1572868
  3.0 0.9 copy-start.5
  4.0 15.3 %copy-start.9 = (bf16[512,512]{1,0:T(8,128)(2,1)S(1)}, bf16[512,512]{1,0:T(8,128)(2,1)}, u32[]{:S(2)}) copy-start(bf16[512,512]{1,0:T(8,128)(2,1)} %param.22) | copy-start | bytes 1572868
  16.6 19.2 %copy-start.6 = (bf16[24,4096]{1,0:T(8,128)(2,1)S(1)}, bf16[24,4096]{1,0:T(8,128)(2,1)}, u32[]{:S(2)}) copy-start(bf16[24,4096]{1,0:T(8,128)(2,1)} %tok_ref.3) | copy-start | bytes 589828
  16.6 19.2 %copy-start.7 = (f32[24,256]{1,0:T(8,128)S(1)}, f32[24,256]{1,0:T(8,128)}, u32[]{:S(2)}) copy-start(f32[24,256]{1,0:T(8,128)} %shift_ref.1) | copy-start | bytes 73732
  35.8 2.8 %copy-start.1 = (f32[24,2,128,256]{3,2,1,0:T(8,128)S(1)}, f32[24,2,128,256]{3,2,1,0:T(8,128)}, u32[]{:S(2)}) copy-start(f32[24,2,128,256]{3,2,1,0:T(8,128)} %state_ref.1) | copy-start | bytes 18874372
  38.6 13.2 %copy-start.8 = (bf16[512,512]{1,0:T(8,128)(2,1)S(1)}, bf16[512,512]{1,0:T(8,128)(2,1)}, u32[]{:S(2)}) copy-start(bf16[512,512]{1,0:T(8,128)(2,1)} %param.27) | copy-start | bytes 1572868
  38.6 39.3 %copy-start.3 = (bf16[1,4096,256]{2,1,0:T(8,128)(2,1)S(1)}, bf16[1,4096,256]{2,1,0:T(8,128)(2,1)}, u32[]{:S(2)}) copy-start(bf16[1,4096,256]{2,1,0:T(8,128)(2,1)} %lin_ref.1) | copy-start | bytes 6291460
  38.6 39.3 %copy-start.4 = (bf16[1,256,4096]{2,1,0:T(8,128)(2,1)S(1)}, bf16[1,256,4096]{2,1,0:T(8,128)(2,1)}, u32[]{:S(2)}) copy-start(bf16[1,256,4096]{2,1,0:T(8,128)(2,1)} %down_ref.1) | copy-start | bytes 6291460
  41.4 36.5 %copy-start.2 = (bf16[1,4096,256]{2,1,0:T(8,128)(2,1)S(1)}, bf16[1,4096,256]{2,1,0:T(8,128)(2,1)}, u32[]{:S(2)}) copy-start(bf16[1,4096,256]{2,1,0:T(8,128)(2,1)} %gate_ref.1) | copy-start | bytes 6291460
